TPU v7x, 32 devices: a whole 2x2x4 slice. The times are simulated.
32 devices in a mesh: sp: 8 (over z, x), tp: 4 (over y, core).
Axes of the slice: x: 2, y: 2, z: 4, core: 2. Of those that a mesh axis runs over, the one named last changes fastest.
Arguments:
- resid: bfloat16 [1024, 2048], P('sp'), may hold values from -8 to 8
- a_val: bfloat16 [1024, 1024], P('sp', 'tp'), may hold values from -8 to 8
- a_gate: bfloat16 [1024, 1024], P('sp', 'tp'), may hold values from -6 to 6
- conv_kernel: bfloat16 [31, 1024], P(None, 'tp'), may hold values from -1 to 1
- conv_bias: float32 [1024], P('tp'), may hold values from -3 to 3
- ln_gain: float32 [1024], P('tp'), may hold values from 0.1 to 1.9
- ln_bias: float32 [1024], P('tp'), may hold values from -3 to 3
- w_out: bfloat16 [1024, 2048], P('tp'), may hold values from -0.1875 to 0.1875
- ffn_gain: float32 [2048], replicated, may hold values from 0.1 to 1.9
- routes: int32 [1024, 4], P('sp'), may hold values from 0 to 7, all different within a row; in each aligned block of 128 rows (0 to 127, 128 to 255, ...) at most 128 rows name the same one
- route_weights: float32 [1024, 4], P('sp'), may hold values from 0.15 to 1.2
- exp_gate: bfloat16 [8, 2048, 4096], P('sp', None, 'tp'), may hold values from -0.125 to 0.125
- exp_up: bfloat16 [8, 2048, 4096], P('sp', None, 'tp'), may hold values from -0.125 to 0.125
- exp_down: bfloat16 [8, 4096, 2048], P('sp', None, 'tp'), may hold values from -0.09375 to 0.09375
- sh_gate: bfloat16 [2048, 512], P(None, 'tp'), may hold values from -0.125 to 0.125
- sh_up: bfloat16 [2048, 512], P(None, 'tp'), may hold values from -0.125 to 0.125
- sh_down: bfloat16 [512, 2048], P(None, 'tp'), may hold values from -0.25 to 0.25
Outputs:
- result: bfloat16 [1024, 2048], P('sp', 'tp')
Inputs may be any that keep to these rules, and one draw needn't show every extreme that they name: `routes`: among the 128 rows of one index of sp, each expert is named at most 128 times, a bound that some block reaches; a row names 4 different experts.
All inputs are finite; a program needn't handle non-finite values.
Results may differ from a plain program's by a relative error of at most 0.007.
Values may be sent and summed in bfloat16 or wider, within the bound.
A program may use at most 64 MiB of HBM per device.

v0:
```python
import jax
import jax.numpy as jnp
from jax import lax
from jax.sharding import PartitionSpec as P

LN_EPS = 1e-05
RMS_EPS = 1e-06


def shifted(value, axis, by):
    size = lax.axis_size(axis)
    pairs = [(i, i + by) for i in range(size) if 0 <= i + by < size]
    return lax.ppermute(value, axis, pairs)


def body_slots(
    resid,
    a_val,
    a_gate,
    conv_kernel,
    conv_bias,
    ln_gain,
    ln_bias,
    w_out,
    ffn_gain,
    routes,
    route_weights,
    exp_gate,
    exp_up,
    exp_down,
    sh_gate,
    sh_up,
    sh_down,
):
    tp_count = lax.axis_size("tp")
    tp_place = lax.axis_index("tp")
    sp_count = lax.axis_size("sp")
    tok_rows = resid.shape[0]
    model_width = resid.shape[1]
    col_width = model_width // tp_count
    col_start = tp_place * col_width
    conv_span = conv_kernel.shape[0]
    channels_all = a_val.shape[1] * tp_count
    gated_in = (a_val.astype(jnp.float32) * jax.nn.sigmoid(a_gate.astype(jnp.float32))).astype(
        jnp.bfloat16
    )
    before = shifted(gated_in[tok_rows - (conv_span - 1) :], "sp", 1)
    padded = jnp.concatenate([before, gated_in], axis=0).astype(jnp.float32)
    kernel = conv_kernel.astype(jnp.float32)

    def add_tap(offset, running):
        window_rows = lax.dynamic_slice_in_dim(padded, offset, tok_rows, 0)
        return running + lax.dynamic_slice_in_dim(kernel, offset, 1, 0) * window_rows

    start_sum = jnp.broadcast_to(conv_bias[None, :], gated_in.shape)
    conv_out = lax.fori_loop(0, conv_span, add_tap, start_sum)
    row_sums = lax.psum((jnp.sum(conv_out, axis=1), jnp.sum(conv_out * conv_out, axis=1)), "tp")
    channel_mean = row_sums[0] / channels_all
    channel_var = row_sums[1] / channels_all - channel_mean * channel_mean
    scaled = (conv_out - channel_mean[:, None]) * lax.rsqrt(
        channel_var[:, None] + LN_EPS
    ) * ln_gain[None, :] + ln_bias[None, :]
    mixed_out = jax.nn.silu(scaled).astype(jnp.bfloat16)
    partial_proj = jnp.dot(mixed_out, w_out, preferred_element_type=jnp.float32)
    projected = lax.psum(partial_proj, "tp")
    middle = (resid.astype(jnp.float32) + projected).astype(jnp.bfloat16)
    middle_f = middle.astype(jnp.float32)
    inverse = lax.rsqrt(jnp.mean(middle_f * middle_f, axis=1, keepdims=True) + RMS_EPS)
    normed = (middle_f * inverse * ffn_gain[None, :]).astype(jnp.bfloat16)
    middle_cols = lax.dynamic_slice_in_dim(middle, col_start, col_width, 1)
    shared_gate = jnp.dot(normed, sh_gate, preferred_element_type=jnp.float32)
    shared_up = jnp.dot(normed, sh_up, preferred_element_type=jnp.float32)
    shared_hidden = (jax.nn.silu(shared_gate) * shared_up).astype(jnp.bfloat16)
    weight_rows = sh_down
    shared = jnp.dot(
        lax.all_gather(shared_hidden, "tp", axis=1, tiled=True),
        weight_rows,
        preferred_element_type=jnp.float32,
    )
    top_count = routes.shape[1]
    local_experts = exp_gate.shape[0]
    experts_all = local_experts * sp_count
    capacity = max(2 * tok_rows * top_count // experts_all, tp_count)
    pair_count = tok_rows * top_count
    chosen = routes.reshape(pair_count)
    one_hot = (chosen[:, None] == jnp.arange(experts_all, dtype=jnp.int32)[None, :]).astype(
        jnp.int32
    )
    earlier = jnp.cumsum(one_hot, axis=0) - one_hot
    place_in = jnp.sum(earlier * one_hot, axis=1)
    slot_of = chosen * capacity + place_in
    owner_ids = (
        jnp.zeros((experts_all * capacity,), jnp.int32)
        .at[slot_of]
        .set(jnp.arange(pair_count, dtype=jnp.int32) + 1)
    )
    owner_grid = owner_ids.reshape(sp_count, local_experts, capacity)
    part_slots = capacity // tp_count
    own_owners = lax.dynamic_slice_in_dim(owner_grid, tp_place * part_slots, part_slots, 2)
    source_row = jnp.maximum(own_owners - 1, 0) // top_count
    taken = normed[source_row.reshape(-1)].reshape(own_owners.shape + (model_width,))
    landed = lax.all_to_all(
        jnp.where((own_owners > 0)[..., None], taken, jnp.zeros((), jnp.bfloat16)),
        "sp",
        split_axis=0,
        concat_axis=0,
        tiled=True,
    )
    arrived = lax.all_gather(landed, "tp", axis=2, tiled=True)
    gate_part = jnp.einsum("sxcd,xdf->sxcf", arrived, exp_gate, preferred_element_type=jnp.float32)
    up_part = jnp.einsum("sxcd,xdf->sxcf", arrived, exp_up, preferred_element_type=jnp.float32)
    expert_hidden = (jax.nn.silu(gate_part) * up_part).astype(jnp.bfloat16)
    weight_rows = exp_down
    expert_sum = jnp.einsum(
        "sxcf,xfd->sxcd",
        lax.all_gather(expert_hidden, "tp", axis=3, tiled=True),
        weight_rows,
        preferred_element_type=jnp.float32,
    )
    expert_out = expert_sum.astype(jnp.bfloat16)
    returned = lax.all_to_all(expert_out, "sp", split_axis=0, concat_axis=0, tiled=True)
    flat_out = returned.reshape(experts_all * capacity, col_width)
    picked = flat_out[slot_of].astype(jnp.float32).reshape(tok_rows, top_count, col_width)
    routed = jnp.sum(picked * route_weights[:, :, None], axis=1)
    return (middle_cols.astype(jnp.float32) + shared + routed).astype(jnp.bfloat16)


def swapped(value, axis, bit):
    size = lax.axis_size(axis)
    return lax.ppermute(value, axis, [(i, i ^ bit) for i in range(size)])


def body_dense(
    resid,
    a_val,
    a_gate,
    conv_kernel,
    conv_bias,
    ln_gain,
    ln_bias,
    w_out,
    ffn_gain,
    routes,
    route_weights,
    exp_gate,
    exp_up,
    exp_down,
    sh_gate,
    sh_up,
    sh_down,
):
    tp_count = lax.axis_size("tp")
    tp_place = lax.axis_index("tp")
    core = tp_place % 2
    row = tp_place // 2
    sp_count = lax.axis_size("sp")
    tok_rows, model_width = resid.shape
    col_width = model_width // tp_count
    half_width = model_width // 2
    part_hidden = exp_gate.shape[2]
    conv_span = conv_kernel.shape[0]
    channels_all = a_val.shape[1] * tp_count
    other_rows = lax.dynamic_slice_in_dim(
        exp_down[0], (1 - row) * 2 * part_hidden, 2 * part_hidden, 0
    )
    swapped_down = swapped(other_rows, "tp", 2)
    gated_in = (a_val.astype(jnp.float32) * jax.nn.sigmoid(a_gate.astype(jnp.float32))).astype(
        jnp.bfloat16
    )
    before = shifted(gated_in[tok_rows - (conv_span - 1) :], "sp", 1)
    expert_ids = jnp.arange(sp_count, dtype=jnp.int32)
    weight_mat = jnp.sum(
        jnp.where(routes[:, :, None] == expert_ids[None, None, :], route_weights[:, :, None], 0.0),
        axis=1,
    )
    weight_all = lax.all_gather(weight_mat, "sp", axis=0, tiled=True)
    weight_own = lax.dynamic_slice_in_dim(weight_all, lax.axis_index("sp"), 1, 1)
    padded = jnp.concatenate([before, gated_in], axis=0).astype(jnp.float32)
    kernel = conv_kernel.astype(jnp.float32)
    conv_out = jnp.broadcast_to(conv_bias[None, :], gated_in.shape)
    for tap in range(conv_span):
        conv_out = conv_out + kernel[tap : tap + 1] * padded[tap : tap + tok_rows]
    row_sums = lax.psum((jnp.sum(conv_out, axis=1), jnp.sum(conv_out * conv_out, axis=1)), "tp")
    channel_mean = row_sums[0] / channels_all
    channel_var = row_sums[1] / channels_all - channel_mean * channel_mean
    scaled = (conv_out - channel_mean[:, None]) * lax.rsqrt(
        channel_var[:, None] + LN_EPS
    ) * ln_gain[None, :] + ln_bias[None, :]
    mixed_out = jax.nn.silu(scaled).astype(jnp.bfloat16)
    partial_proj = jnp.dot(mixed_out, w_out, preferred_element_type=jnp.float32)
    give = lax.dynamic_slice_in_dim(partial_proj, (1 - core) * half_width, half_width, 1)
    keep = lax.dynamic_slice_in_dim(partial_proj, core * half_width, half_width, 1)
    chip_sum = keep + swapped(give.astype(jnp.bfloat16), "tp", 1).astype(jnp.float32)
    chip_sum = chip_sum.astype(jnp.bfloat16)
    half_sum = chip_sum.astype(jnp.float32) + swapped(chip_sum, "tp", 2).astype(jnp.float32)
    resid_half = lax.dynamic_slice_in_dim(resid, core * half_width, half_width, 1)
    mid_half = (resid_half.astype(jnp.float32) + half_sum).astype(jnp.bfloat16)
    mid_all = lax.all_gather(mid_half, "sp", axis=0, tiled=True)
    mid_peer = swapped(mid_half, "tp", 1)
    first = jnp.where(core == 0, mid_half, mid_peer)
    second = jnp.where(core == 0, mid_peer, mid_half)
    middle = jnp.concatenate([first, second], axis=1)
    middle_f = middle.astype(jnp.float32)
    inverse = lax.rsqrt(jnp.mean(middle_f * middle_f, axis=1, keepdims=True) + RMS_EPS)
    normed = (middle_f * inverse * ffn_gain[None, :]).astype(jnp.bfloat16)
    middle_cols = lax.dynamic_slice_in_dim(middle, tp_place * col_width, col_width, 1)
    shared_gate = jnp.dot(normed, sh_gate, preferred_element_type=jnp.float32)
    shared_up = jnp.dot(normed, sh_up, preferred_element_type=jnp.float32)
    shared_hidden = (jax.nn.silu(shared_gate) * shared_up).astype(jnp.bfloat16)
    shared = jnp.dot(
        lax.all_gather(shared_hidden, "tp", axis=1, tiled=True),
        sh_down,
        preferred_element_type=jnp.float32,
    )
    mid_all_peer = swapped(mid_all, "tp", 1)
    rows_first = jnp.where(core == 0, mid_all, mid_all_peer)
    rows_second = jnp.where(core == 0, mid_all_peer, mid_all)
    rows_f = jnp.concatenate([rows_first, rows_second], axis=1).astype(jnp.float32)
    rows_inverse = lax.rsqrt(jnp.mean(rows_f * rows_f, axis=1, keepdims=True) + RMS_EPS)
    rows = (rows_f * rows_inverse * ffn_gain[None, :]).astype(jnp.bfloat16)
    gate_part = jnp.dot(rows, exp_gate[0], preferred_element_type=jnp.float32)
    up_part = jnp.dot(rows, exp_up[0], preferred_element_type=jnp.float32)
    hidden = (jax.nn.silu(gate_part) * up_part).astype(jnp.bfloat16)
    hidden_peer = swapped(hidden, "tp", 1)
    own_at = tp_place * part_hidden
    peer_at = (tp_place ^ 1) * part_hidden
    stay = lax.dynamic_slice_in_dim
    out_own = jnp.dot(
        hidden, stay(exp_down[0], own_at, part_hidden, 0), preferred_element_type=jnp.float32
    ) + jnp.dot(
        hidden_peer, stay(exp_down[0], peer_at, part_hidden, 0), preferred_element_type=jnp.float32
    )
    out_far = jnp.dot(
        hidden,
        stay(swapped_down, core * part_hidden, part_hidden, 0),
        preferred_element_type=jnp.float32,
    ) + jnp.dot(
        hidden_peer,
        stay(swapped_down, (1 - core) * part_hidden, part_hidden, 0),
        preferred_element_type=jnp.float32,
    )
    both = jnp.concatenate([out_own * weight_own, out_far * weight_own], axis=1).astype(
        jnp.bfloat16
    )
    summed = lax.psum_scatter(both, "sp", scatter_dimension=0, tiled=True)
    far = swapped(summed[:, col_width:], "tp", 2)
    routed = summed[:, :col_width].astype(jnp.float32) + far.astype(jnp.float32)
    return (middle_cols.astype(jnp.float32) + shared + routed).astype(jnp.bfloat16)


def body(*args):
    tok_rows = args[0].shape[0]
    top_count = args[9].shape[1]
    local_experts = args[11].shape[0]
    experts_all = local_experts * lax.axis_size("sp")
    capacity = 2 * tok_rows * top_count // experts_all
    if local_experts == 1 and lax.axis_size("tp") == 4 and (capacity >= tok_rows):
        return body_dense(*args)
    return body_slots(*args)


def solution(mesh):
    in_specs = (
        P("sp", None),
        P("sp", "tp"),
        P("sp", "tp"),
        P(None, "tp"),
        P("tp"),
        P("tp"),
        P("tp"),
        P("tp", None),
        P(),
        P("sp", None),
        P("sp", None),
        P("sp", None, "tp"),
        P("sp", None, "tp"),
        P("sp", None, "tp"),
        P(None, "tp"),
        P(None, "tp"),
        P(None, "tp"),
    )
    out_specs = P("sp", "tp")
    return jax.shard_map(body, mesh=mesh, in_specs=in_specs, out_specs=out_specs, check_vma=False)
```

profile of v0, /device:TPU:0, one launch (start us, length us, event | category | flops | bytes accessed | tf_op | source)
XLA Modules:
  0.0 230.6 jit_solution(7663626764208417222)
XLA Ops:
  6.5 1.0 multiply_convert_fusion.4
  7.6 4.9 %collective-permute-start = (bf16[30,256]{1,0:T(8,128)(2,1)S(1)}, bf16[30,256]{1,0:T(8,128)(2,1)S(1)}, u32[]{:S(2)}, u32[]{:S(2)}) collective-permute-start(bf16[30,256]{1,0:T(8,128)(2,1)S(1)} %slice.261), channel_id=1, source_target_pairs={{0,4},{4,8},{8,12},{12,16},{16,20},{20,24},{24,28},{1,5},{5,9},{9,... | collective-permute-start | bytes 46088 | tf_op jit(solution)/shard_map/ppermute | solution.py:13
  12.4 1.0 fusion.73
  13.5 1.0 fusion.74
  14.5 1.3 fusion.71
  15.8 6.3 %all-reduce = (f32[128]{0:T(128)S(1)}, f32[128]{0:T(128)S(1)}) all-reduce(f32[128]{0:T(128)S(1)} %get-tuple-element.6, f32[128]{0:T(128)S(1)} %get-tuple-element.5), channel_id=1, replica_groups=mesh['sp'=8,'tp'=4] {'tp'}, use_global_device_ids=true, to_apply=%region_3.4 | all-reduce | flops 256 | bytes 2048 | tf_op jit(solution)/shard_map/psum | solution.py:183
  22.2 0.4 fusion.51
  22.6 0.1 collective-permute-start.1
  22.7 1.5 collective-permute-done.1
  24.2 0.1 add_convert_fusion.1
  24.3 1.1 collective-permute-start.2
  25.4 7.3 %collective-permute-done.2 = bf16[128,1024]{1,0:T(8,128)(2,1)S(1)} collective-permute-done((bf16[128,1024]{1,0:T(8,128)(2,1)S(1)}, bf16[128,1024]{1,0:T(8,128)(2,1)S(1)}, u32[]{:S(2)}, u32[]{:S(2)}) %collective-permute-start.2) | collective-permute-done | bytes 262176 | tf_op jit(solution)/shard_map/ppermute | solution.py:130
  32.7 0.8 add_convert_fusion
  33.5 0.0 all-gather.2.cloned.1.call-update
  33.6 0.0 reduce-scatter.2.cloned.1.call-start
  33.6 50.1 %all-gather.2.cloned.1.call-done = bf16[1024,1024]{1,0:T(8,128)(2,1)} async-done(((bf16[128,1024]{1,0:T(8,128)(2,1)}), bf16[1024,1024]{1,0:T(8,128)(2,1)}) %all-gather.2.cloned.1.call-update) | async-done | bytes 2097168 | tf_op jit(solution)/shard_map/all_gather | solution.py:198
  83.8 1.7 dynamic-slice_bitcast_fusion
  85.5 1.5 collective-permute-start.6
  87.0 1.2 collective-permute-done.4
  88.3 2.5 %broadcast_select_fusion.1 = (bf16[1024,1024]{1,0:T(8,128)(2,1)S(1)}, bf16[1024,1024]{1,0:T(8,128)(2,1)S(1)}) fusion(bf16[1024,1024]{1,0:T(8,128)(2,1)} %all-gather.2.cloned.1.call-done, bf16[1024,1024]{1,0:T(8,128)(2,1)} %collective-permute-done.4, pred[]{:T(512)S(6)} %eq.10), kind=kLoop, calls=%fused_computation.16 | loop fusion | flops 2097152 | bytes 8388609 | tf_op jit(solution)/shard_map/jit(_where)/select_n | solution.py:216
  90.8 0.0 copy-start.8
  90.8 1.0 fusion
  91.8 1.2 copy-done.8
  92.9 4.6 %fusion.5 = f32[1024,1024]{1,0:T(8,128)S(1)} fusion(bf16[1,2048,1024]{2,1,0:T(8,128)(2,1)S(1)} %copy-done.8, f32[2048]{0:T(1024)S(1)} %copy-done.11, f32[1024]{0:T(1024)S(1)} %add_rsqrt_fusion, bf16[1024,1024]{1,0:T(8,128)(2,1)S(1)} %get-tuple-element.11, bf16[1024,1024]{1,0:T(8,128)(2,1)S(1)} %get-tuple-element.10), kind=kOutput, calls=%fused_computation.8 | convolution fusion | flops 4309647360 | bytes 12595200 | tf_op jit(solution)/shard_map/dot_general | solution.py:221
  97.5 0.0 copy-start.4
  97.5 0.0 copy-start.5
  97.5 6.4 %multiply_convert_fusion = bf16[1024,1024]{1,0:T(8,128)(2,1)} fusion(f32[1024,1024]{1,0:T(8,128)S(1)} %fusion.5, bf16[1,2048,1024]{2,1,0:T(8,128)(2,1)S(1)} %copy-done.9, f32[2048]{0:T(1024)S(1)} %copy-done.11, f32[1024]{0:T(1024)S(1)} %add_rsqrt_fusion, bf16[1024,1024]{1,0:T(8,128)(2,1)S(1)} %get-tuple-element.11, bf16[1024,1024]{1,0:T(8,128)(2,1)S(1)} %get-tuple-element.10), kind=kOutput, calls=%fused_computation.10 | convolution fusion | flops 4315938816 | bytes 14692352 | tf_op jit(solution)/shard_map/dot_general | solution.py:222
  103.9 0.1 collective-permute-start.5
  104.1 30.8 %all_gather.11 = f32[1024,8]{0,1:T(8,128)S(1)} all-gather(f32[128,8]{0,1:T(8,128)S(1)} %select_reduce_fusion), channel_id=1, replica_groups=mesh['sp'=8,'tp'=4] {'sp'}, dimensions={0}, use_global_device_ids=true | all-gather | bytes 36864 | tf_op jit(solution)/shard_map/all_gather | solution.py:176
  134.9 3.1 %fusion.12 = f32[1024,512]{1,0:T(8,128)S(1)} fusion(bf16[1024,1024]{1,0:T(8,128)(2,1)} %multiply_convert_fusion, bf16[1,4096,512]{2,1,0:T(8,128)(2,1)} %param.30, s32[]{:T(128)S(6)} %select_n.73), kind=kOutput, calls=%fused_computation.25 | convolution fusion | flops 1073741824 | bytes 5242884 | tf_op jit(solution)/shard_map/dot_general | solution.py:228
  138.0 3.1 %fusion.14 = f32[1024,512]{1,0:T(8,128)S(1)} fusion(bf16[1024,1024]{1,0:T(8,128)(2,1)} %collective-permute-done.5, bf16[2048,512]{1,0:T(8,128)(2,1)} %collective-permute-done.6, s32[]{:T(128)S(6)} %select_n.66), kind=kOutput, calls=%fused_computation.27 | convolution fusion | flops 1073741824 | bytes 5242884 | tf_op jit(solution)/shard_map/dot_general | solution.py:237
  141.1 3.1 %multiply_convert_fusion.1 = bf16[1024,512]{1,0:T(8,128)(2,1)S(1)} fusion(f32[1024,512]{1,0:T(8,128)S(1)} %fusion.14, bf16[1024,1024]{1,0:T(8,128)(2,1)} %multiply_convert_fusion, bf16[2048,512]{1,0:T(8,128)(2,1)} %collective-permute-done.6, s32[]{:T(128)S(6)} %select_n.65, f32[1024]{0:T(1024)S(1)} %bitcast.88), kind=kOutput, calls=%fused_computation.12 | convolution fusion | flops 1075314688 | bytes 6295556 | tf_op jit(solution)/shard_map/dot_general | solution.py:233
  144.2 3.1 %multiply_convert_fusion.2 = bf16[1024,512]{1,0:T(8,128)(2,1)S(1)} fusion(f32[1024,512]{1,0:T(8,128)S(1)} %fusion.12, bf16[1024,1024]{1,0:T(8,128)(2,1)} %collective-permute-done.5, f32[1024]{0:T(1024)S(1)} %bitcast.89, bf16[1,4096,512]{2,1,0:T(8,128)(2,1)} %param.30, s32[]{:T(128)S(6)} %select_n.74), kind=kOutput, calls=%fused_computation.14 | convolution fusion | flops 1075314688 | bytes 6295556 | tf_op jit(solution)/shard_map/dot_general | solution.py:230
  147.4 0.0 copy-start.10
  147.4 1.6 pad_maximum_fusion.1
  149.0 0.0 reduce-scatter.2.cloned.1.call-update
  149.0 0.1 collective-permute-start.3
  149.1 1.5 collective-permute-done.3
  150.7 0.2 fusion.8
  150.9 0.4 fusion.63
  151.2 1.4 fusion.7
  152.6 5.4 %all_gather.9 = bf16[128,512]{1,0:T(8,128)(2,1)S(1)} all-gather(bf16[128,128]{1,0:T(8,128)(2,1)S(1)} %fusion.7), channel_id=1, replica_groups=mesh['sp'=8,'tp'=4] {'tp'}, dimensions={1}, use_global_device_ids=true | all-gather | bytes 163840 | tf_op jit(solution)/shard_map/all_gather | solution.py:211
  158.1 58.0 %reduce-scatter.2.cloned.1.call-done = bf16[128,1024]{1,0:T(8,128)(2,1)} async-done(((bf16[1024,1024]{1,0:T(8,128)(2,1)}), bf16[128,1024]{1,0:T(8,128)(2,1)}) %reduce-scatter.2.cloned.1.call-update) | async-done | bytes 262160 | tf_op jit(solution)/shard_map/reduce_scatter | solution.py:245
  216.1 0.9 slice.324
  217.0 1.5 collective-permute-start.7
  218.5 0.2 fusion.75
  218.8 3.3 %collective-permute-done.7 = bf16[128,512]{1,0:T(8,128)(2,1)S(1)} collective-permute-done((bf16[128,512]{1,0:T(8,128)(2,1)S(1)}, bf16[128,512]{1,0:T(8,128)(2,1)S(1)}, u32[]{:S(2)}, u32[]{:S(2)}) %collective-permute-start.7) | collective-permute-done | bytes 131104 | tf_op jit(solution)/shard_map/ppermute | solution.py:130
  222.0 1.7 add_convert_fusion.2
  (33 shorter events, 0.2 us)
Async XLA Ops:
  6.5 15.6 %copy-start = (bf16[256,2048]{1,0:T(8,128)(2,1)S(1)}, bf16[256,2048]{1,0:T(8,128)(2,1)}, u32[]{:S(2)}) copy-start(bf16[256,2048]{1,0:T(8,128)(2,1)} %param.24) | copy-start | bytes 3145732
  6.5 15.6 %copy-start.6 = (f32[256]{0:T(256)S(1)}, f32[256]{0:T(256)}, u32[]{:S(2)}) copy-start(f32[256]{0:T(256)} %param.23) | copy-start | bytes 3076
  6.5 15.7 %copy-start.7 = (f32[256]{0:T(256)S(1)}, f32[256]{0:T(256)}, u32[]{:S(2)}) copy-start(f32[256]{0:T(256)} %param.22) | copy-start | bytes 3076
  6.5 77.2 %all-gather.2.cloned.1.call-start = ((), (), s32[]{:S(2)}) async-start(), calls=%async_computation.1 | async-start | bytes 2359296 | tf_op jit(solution)/shard_map/all_gather | solution.py:198
  7.6 6.9 %collective-permute-start = (bf16[30,256]{1,0:T(8,128)(2,1)S(1)}, bf16[30,256]{1,0:T(8,128)(2,1)S(1)}, u32[]{:S(2)}, u32[]{:S(2)}) collective-permute-start(bf16[30,256]{1,0:T(8,128)(2,1)S(1)} %slice.261), channel_id=1, source_target_pairs={{0,4},{4,8},{8,12},{12,16},{16,20},{20,24},{24,28},{1,5},{5,9},{9,... | collective-permute-start | bytes 46088 | tf_op jit(solution)/shard_map/ppermute | solution.py:13
  14.5 18.3 %copy-start.3 = (bf16[128,2048]{1,0:T(8,128)(2,1)S(1)}, bf16[128,2048]{1,0:T(8,128)(2,1)}, u32[]{:S(2)}) copy-start(bf16[128,2048]{1,0:T(8,128)(2,1)} %param.17) | copy-start | bytes 1572868
  22.6 1.6 collective-permute-start.1
  24.3 8.4 %collective-permute-start.2 = (bf16[128,1024]{1,0:T(8,128)(2,1)S(1)}, bf16[128,1024]{1,0:T(8,128)(2,1)S(1)}, u32[]{:S(2)}, u32[]{:S(2)}) collective-permute-start(bf16[128,1024]{1,0:T(8,128)(2,1)S(1)} %add_convert_fusion.1), channel_id=1, source_target_pairs={{0,2},{1,3},{2,0},{3,1},{4,6},{5,7},{6,4},{7,5},{8,10},{9,11},{10,... | collective-permute-start | bytes 786440 | tf_op jit(solution)/shard_map/ppermute | solution.py:130
  33.6 182.5 %reduce-scatter.2.cloned.1.call-start = ((), (), s32[]{:S(2)}) async-start(), calls=%async_computation.2 | async-start | bytes 2359296 | tf_op jit(solution)/shard_map/reduce_scatter | solution.py:245
  83.8 4.5 %collective-permute-start.4 = (bf16[1024,1024]{1,0:T(8,128)(2,1)}, bf16[1024,1024]{1,0:T(8,128)(2,1)}, u32[]{:S(2)}, u32[]{:S(2)}) collective-permute-start(bf16[1024,1024]{1,0:T(8,128)(2,1)} %all-gather.2.cloned.1.call-done), channel_id=1, source_target_pairs={{0,1},{1,0},{2,3},{3,2},{4,5},{5,4},{6,7},{7,6},{8,9},{9,8},{10,11... | collective-permute-start | bytes 6291464 | tf_op jit(solution)/shard_map/ppermute | solution.py:130
  85.5 52.5 %collective-permute-start.6 = (bf16[2048,512]{1,0:T(8,128)(2,1)S(1)}, bf16[2048,512]{1,0:T(8,128)(2,1)}, u32[]{:S(2)}, u32[]{:S(2)}) collective-permute-start(bf16[2048,512]{1,0:T(8,128)(2,1)S(1)} %dynamic-slice_bitcast_fusion), channel_id=1, source_target_pairs={{0,2},{1,3},{2,0},{3,1},{4,6},{5,7},{6,4},{7,5},{8,10},{9,11},{10,... | collective-permute-start | bytes 6291464 | tf_op jit(solution)/shard_map/ppermute | solution.py:130
  90.8 2.2 copy-start.8
  90.8 2.2 copy-start.11
  92.9 4.6 %copy-start.9 = (bf16[1,2048,1024]{2,1,0:T(8,128)(2,1)S(1)}, bf16[1,2048,1024]{2,1,0:T(8,128)(2,1)}, u32[]{:S(2)}) copy-start(bf16[1,2048,1024]{2,1,0:T(8,128)(2,1)} %param.29) | copy-start | bytes 12582916
  97.5 6.5 %copy-start.4 = (f32[128,4]{0,1:T(4,128)S(1)}, f32[128,4]{0,1:T(4,128)}, u32[]{:S(2)}) copy-start(f32[128,4]{0,1:T(4,128)} %param.27) | copy-start | bytes 6148
  97.5 6.5 %copy-start.5 = (s32[128,4]{0,1:T(4,128)S(1)}, s32[128,4]{0,1:T(4,128)}, u32[]{:S(2)}) copy-start(s32[128,4]{0,1:T(4,128)} %param.26) | copy-start | bytes 6148
  103.9 34.1 %collective-permute-start.5 = (bf16[1024,1024]{1,0:T(8,128)(2,1)}, bf16[1024,1024]{1,0:T(8,128)(2,1)}, u32[]{:S(2)}, u32[]{:S(2)}) collective-permute-start(bf16[1024,1024]{1,0:T(8,128)(2,1)} %multiply_convert_fusion), channel_id=1, source_target_pairs={{0,1},{1,0},{2,3},{3,2},{4,5},{5,4},{6,7},{7,6},{8,9},{9,8},{10,11... | collective-permute-start | bytes 6291464 | tf_op jit(solution)/shard_map/ppermute | solution.py:130
  147.4 1.6 copy-start.1
  147.4 3.5 %copy-start.10 = (bf16[2048,128]{1,0:T(8,128)(2,1)S(1)}, bf16[2048,128]{1,0:T(8,128)(2,1)}, u32[]{:S(2)}) copy-start(bf16[2048,128]{1,0:T(8,128)(2,1)} %param.31) | copy-start | bytes 1572868
  149.0 69.6 %copy-start.2 = (bf16[512,512]{1,0:T(8,128)(2,1)S(1)}, bf16[512,512]{1,0:T(8,128)(2,1)}, u32[]{:S(2)}) copy-start(bf16[512,512]{1,0:T(8,128)(2,1)} %param.33) | copy-start | bytes 1572868
  149.0 1.6 collective-permute-start.3
  217.0 5.0 %collective-permute-start.7 = (bf16[128,512]{1,0:T(8,128)(2,1)S(1)}, bf16[128,512]{1,0:T(8,128)(2,1)S(1)}, u32[]{:S(2)}, u32[]{:S(2)}) collective-permute-start(bf16[128,512]{1,0:T(8,128)(2,1)S(1)} %slice.324), channel_id=1, source_target_pairs={{0,2},{1,3},{2,0},{3,1},{4,6},{5,7},{6,4},{7,5},{8,10},{9,11},{10,... | collective-permute-start | bytes 393224 | tf_op jit(solution)/shard_map/ppermute | solution.py:130
Sparse Core Ops, SparseCore 0:
  33.7 50.0 all-gather.1
  149.1 66.9 reduce-scatter.1
where the time goes:
time: 231 us
  waiting for transfers between devices  123 us (53%)
  blocking collectives  42.6 us (18%)
  matrix products  25.8 us (11%)
  between operations  13.7 us (6%)
  other arithmetic  10.3 us (4%)
  starting transfers between devices  9.37 us (4%)
  local copies, waits for them, and re-layouts  5.9 us (3%)
    reduce_scatter x1, waiting for transfers between devices, body_dense(): summed = lax.psum_scatter(both, 'sp', scatter_dimension=0, tiled=True)  58 us
    all_gather x1, waiting for transfers between devices, body_dense(): mid_all = lax.all_gather(mid_half, 'sp', axis=0, tiled=True)  50.1 us
    all_gather x1, blocking collectives, body_dense(): weight_all = lax.all_gather(weight_mat, 'sp', axis=0, tiled=True)  30.8 us
    ppermute x7, waiting for transfers between devices, swapped(): return lax.ppermute(value, axis, [(i, i ^ bit) for i in range(size)])  14.8 us
    dot_general x1, matrix products, body_dense(): up_part = jnp.dot(rows, exp_up[0], preferred_element_type=jnp.float32)  6.37 us
    psum x1, blocking collectives, body_dense(): lax.psum((jnp.sum(conv_out, axis=1), jnp.sum(conv_out * conv_out, axis=1)...  6.33 us
    all_gather x1, blocking collectives, body_dense(): lax.all_gather(shared_hidden, 'tp', axis=1, tiled=True)  5.45 us
    ppermute x1, starting transfers between devices, shifted(): return lax.ppermute(value, axis, pairs)  4.87 us
  transfers between devices with their start and end apart: 10, of which 7 were waited for; matrix products, arithmetic and copies ran while one was open for 10% of the time, Pallas kernels for 0%

commit v1 on v0

--- a/solution.py
+++ b/solution.py
@@ -195,7 +195,12 @@
     half_sum = chip_sum.astype(jnp.float32) + swapped(chip_sum, "tp", 2).astype(jnp.float32)
     resid_half = lax.dynamic_slice_in_dim(resid, core * half_width, half_width, 1)
     mid_half = (resid_half.astype(jnp.float32) + half_sum).astype(jnp.bfloat16)
-    mid_all = lax.all_gather(mid_half, "sp", axis=0, tiled=True)
+    ring = [mid_half]
+    for hop in range(7):
+        ring.append(lax.ppermute(ring[-1], "sp", [(dev, (dev + 1) % 8) for dev in range(8)]))
+    mid_all = jnp.roll(
+        jnp.concatenate(ring[::-1], axis=0), (lax.axis_index("sp") + 1) * ring[0].shape[0], axis=0
+    )
     mid_peer = swapped(mid_half, "tp", 1)
     first = jnp.where(core == 0, mid_half, mid_peer)
     second = jnp.where(core == 0, mid_peer, mid_half)

time: 231 us -> 251 us (1.087)
  waiting for transfers between devices: 123 us -> 137 us
  local copies, waits for them, and re-layouts: 5.9 us -> 12.6 us
    ppermute x0 -> x7, waiting for transfers between devices: none -> 65.6 us  [body_dense(): lax.ppermute(ring[-1], 'sp', [(dev, (dev + 1) % 8) for dev in range(8)])]
    all_gather x1 -> x0, waiting for transfers between devices: 50.1 us -> none  [body_dense(): mid_all = lax.all_gather(mid_half, 'sp', axis=0, tiled=True)]
    unnamed x24 -> x44, local copies, waits for them, and re-layouts: 1.23 us -> 4.9 us
    ppermute x7, waiting for transfers between devices: 14.8 us -> 12.3 us  [swapped(): return lax.ppermute(value, axis, [(i, i ^ bit) for i in range(size)])]
  transfers between devices with their start and end apart: 10 -> 16, of which waited for: 7 -> 12; matrix products, arithmetic and copies ran while one was open for 10% -> 10% of each run, Pallas kernels for 0% -> 0%
where the time goes in v1:
time: 251 us
  waiting for transfers between devices  137 us (55%)
  blocking collectives  42.6 us (17%)
  matrix products  24.8 us (10%)
  between operations  13.8 us (5%)
  local copies, waits for them, and re-layouts  12.6 us (5%)
  starting transfers between devices  10.4 us (4%)
  other arithmetic  9.96 us (4%)
    ppermute x7, waiting for transfers between devices, body_dense(): lax.ppermute(ring[-1], 'sp', [(dev, (dev + 1) % 8) for dev in range(8)])  65.6 us
    reduce_scatter x1, waiting for transfers between devices, body_dense(): summed = lax.psum_scatter(both, 'sp', scatter_dimension=0, tiled=True)  58.9 us
    all_gather x1, blocking collectives, body_dense(): weight_all = lax.all_gather(weight_mat, 'sp', axis=0, tiled=True)  30.8 us
    ppermute x7, waiting for transfers between devices, swapped(): return lax.ppermute(value, axis, [(i, i ^ bit) for i in range(size)])  12.3 us
    dot_general x1, matrix products, body_dense(): up_part = jnp.dot(rows, exp_up[0], preferred_element_type=jnp.float32)  6.37 us
    psum x1, blocking collectives, body_dense(): lax.psum((jnp.sum(conv_out, axis=1), jnp.sum(conv_out * conv_out, axis=1)...  6.33 us
    all_gather x1, blocking collectives, body_dense(): lax.all_gather(shared_hidden, 'tp', axis=1, tiled=True)  5.45 us
  transfers between devices with their start and end apart: 16, of which 12 were waited for; matrix products, arithmetic and copies ran while one was open for 10% of the time, Pallas kernels for 0%

profile of v1, /device:TPU:0, one launch (start us, length us, event | category | flops | bytes accessed | tf_op | source)
XLA Modules:
  0.0 250.9 jit_solution(8320756707108558402)
XLA Ops:
  6.5 1.0 multiply_convert_fusion.4
  7.6 4.9 %collective-permute-start = (bf16[30,256]{1,0:T(8,128)(2,1)S(1)}, bf16[30,256]{1,0:T(8,128)(2,1)S(1)}, u32[]{:S(2)}, u32[]{:S(2)}) collective-permute-start(bf16[30,256]{1,0:T(8,128)(2,1)S(1)} %slice.261), channel_id=1, source_target_pairs={{0,4},{4,8},{8,12},{12,16},{16,20},{20,24},{24,28},{1,5},{5,9},{9,... | collective-permute-start | bytes 46088 | tf_op jit(solution)/shard_map/ppermute | solution.py:13
  12.4 1.0 fusion.73
  13.5 1.0 fusion.74
  14.5 1.3 fusion.71
  15.8 6.3 %all-reduce = (f32[128]{0:T(128)S(1)}, f32[128]{0:T(128)S(1)}) all-reduce(f32[128]{0:T(128)S(1)} %get-tuple-element.6, f32[128]{0:T(128)S(1)} %get-tuple-element.5), channel_id=1, replica_groups=mesh['sp'=8,'tp'=4] {'tp'}, use_global_device_ids=true, to_apply=%region_3.4 | all-reduce | flops 256 | bytes 2048 | tf_op jit(solution)/shard_map/psum | solution.py:183
  22.2 0.4 fusion.51
  22.7 1.5 collective-permute-done.1
  24.3 1.1 collective-permute-start.2
  25.4 7.3 %collective-permute-done.2 = bf16[128,1024]{1,0:T(8,128)(2,1)S(1)} collective-permute-done((bf16[128,1024]{1,0:T(8,128)(2,1)S(1)}, bf16[128,1024]{1,0:T(8,128)(2,1)S(1)}, u32[]{:S(2)}, u32[]{:S(2)}) %collective-permute-start.2) | collective-permute-done | bytes 262176 | tf_op jit(solution)/shard_map/ppermute | solution.py:130
  32.7 0.1 add_convert_fusion
  32.8 1.6 collective-permute-start.4
  34.5 8.6 %collective-permute-done.4 = bf16[128,1024]{1,0:T(8,128)(2,1)S(1)} collective-permute-done((bf16[128,1024]{1,0:T(8,128)(2,1)S(1)}, bf16[128,1024]{1,0:T(8,128)(2,1)S(1)}, u32[]{:S(2)}, u32[]{:S(2)}) %collective-permute-start.4) | collective-permute-done | bytes 262176 | tf_op jit(solution)/shard_map/ppermute | solution.py:200
  43.1 9.3 %collective-permute-done.5 = bf16[128,1024]{1,0:T(8,128)(2,1)S(1)} collective-permute-done((bf16[128,1024]{1,0:T(8,128)(2,1)S(1)}, bf16[128,1024]{1,0:T(8,128)(2,1)S(1)}, u32[]{:S(2)}, u32[]{:S(2)}) %collective-permute-start.5) | collective-permute-done | bytes 262176 | tf_op jit(solution)/shard_map/ppermute | solution.py:200
  52.4 9.1 %collective-permute-done.6 = bf16[128,1024]{1,0:T(8,128)(2,1)S(1)} collective-permute-done((bf16[128,1024]{1,0:T(8,128)(2,1)S(1)}, bf16[128,1024]{1,0:T(8,128)(2,1)S(1)}, u32[]{:S(2)}, u32[]{:S(2)}) %collective-permute-start.6) | collective-permute-done | bytes 262176 | tf_op jit(solution)/shard_map/ppermute | solution.py:200
  61.5 9.1 %collective-permute-done.7 = bf16[128,1024]{1,0:T(8,128)(2,1)S(1)} collective-permute-done((bf16[128,1024]{1,0:T(8,128)(2,1)S(1)}, bf16[128,1024]{1,0:T(8,128)(2,1)S(1)}, u32[]{:S(2)}, u32[]{:S(2)}) %collective-permute-start.7) | collective-permute-done | bytes 262176 | tf_op jit(solution)/shard_map/ppermute | solution.py:200
  70.6 9.7 %collective-permute-done.8 = bf16[128,1024]{1,0:T(8,128)(2,1)S(1)} collective-permute-done((bf16[128,1024]{1,0:T(8,128)(2,1)S(1)}, bf16[128,1024]{1,0:T(8,128)(2,1)S(1)}, u32[]{:S(2)}, u32[]{:S(2)}) %collective-permute-start.8) | collective-permute-done | bytes 262176 | tf_op jit(solution)/shard_map/ppermute | solution.py:200
  80.2 10.8 %collective-permute-done.9 = bf16[128,1024]{1,0:T(8,128)(2,1)S(1)} collective-permute-done((bf16[128,1024]{1,0:T(8,128)(2,1)S(1)}, bf16[128,1024]{1,0:T(8,128)(2,1)S(1)}, u32[]{:S(2)}, u32[]{:S(2)}) %collective-permute-start.9) | collective-permute-done | bytes 262176 | tf_op jit(solution)/shard_map/ppermute | solution.py:200
  91.0 9.1 %collective-permute-done.10 = bf16[128,1024]{1,0:T(8,128)(2,1)S(1)} collective-permute-done((bf16[128,1024]{1,0:T(8,128)(2,1)S(1)}, bf16[128,1024]{1,0:T(8,128)(2,1)S(1)}, u32[]{:S(2)}, u32[]{:S(2)}) %collective-permute-start.10) | collective-permute-done | bytes 262176 | tf_op jit(solution)/shard_map/ppermute | solution.py:200
  100.3 0.5 copy-done.3
  100.9 1.0 constant_dynamic-update-slice_fusion.7
  102.1 1.9 copy-done.1
  104.0 1.5 constant_dynamic-slice_fusion.1
  105.5 3.2 %dynamic-slice_bitcast_fusion = bf16[2048,512]{1,0:T(8,128)(2,1)} fusion(bf16[1,4096,512]{2,1,0:T(8,128)(2,1)} %param.30, s32[]{:T(128)S(6)} %select_n.92), kind=kLoop, calls=%fused_computation.13 | loop fusion | bytes 4194308 | tf_op jit(solution)/shard_map/dynamic_slice | solution.py:163
  108.8 1.0 collective-permute-start.13
  109.8 0.2 collective-permute-done.11
  110.0 2.8 %broadcast_select_fusion.1 = (bf16[1024,1024]{1,0:T(8,128)(2,1)S(1)}, bf16[1024,1024]{1,0:T(8,128)(2,1)S(1)}) fusion(bf16[1024,1024]{1,0:T(8,128)(2,1)} %collective-permute-done.11, pred[]{:T(512)S(6)} %eq.13, bf16[2048,1024]{1,0:T(8,128)(2,1)S(1)} %copy-done.2, s32[]{:T(128)S(6)} %select_n.84), kind=kLoop, calls=%fused_computation.16 | loop fusion | flops 2097152 | bytes 8388613 | tf_op jit(solution)/shard_map/jit(_where)/select_n | solution.py:221
  112.9 1.0 fusion
  113.9 1.2 copy-done.10
  115.1 4.6 %fusion.5 = f32[1024,1024]{1,0:T(8,128)S(1)} fusion(bf16[1,2048,1024]{2,1,0:T(8,128)(2,1)S(1)} %copy-done.10, f32[2048]{0:T(1024)S(1)} %copy-done.14, f32[1024]{0:T(1024)S(1)} %add_rsqrt_fusion, bf16[1024,1024]{1,0:T(8,128)(2,1)S(1)} %get-tuple-element.11, bf16[1024,1024]{1,0:T(8,128)(2,1)S(1)} %get-tuple-element.10), kind=kOutput, calls=%fused_computation.8 | convolution fusion | flops 4309647360 | bytes 12595200 | tf_op jit(solution)/shard_map/dot_general | solution.py:226
  119.7 6.4 %multiply_convert_fusion = bf16[1024,1024]{1,0:T(8,128)(2,1)} fusion(f32[1024,1024]{1,0:T(8,128)S(1)} %fusion.5, bf16[1,2048,1024]{2,1,0:T(8,128)(2,1)S(1)} %copy-done.11, f32[2048]{0:T(1024)S(1)} %copy-done.14, f32[1024]{0:T(1024)S(1)} %add_rsqrt_fusion, bf16[1024,1024]{1,0:T(8,128)(2,1)S(1)} %get-tuple-element.11, ...), kind=kOutput, calls=%fused_computation.10 | convolution fusion | flops 4315938816 | bytes 14692352 | tf_op jit(solution)/shard_map/dot_general | solution.py:227
  126.1 0.1 collective-permute-start.12
  126.2 30.8 %all_gather.7 = f32[1024,8]{0,1:T(8,128)S(1)} all-gather(f32[128,8]{0,1:T(8,128)S(1)} %select_reduce_fusion), channel_id=1, replica_groups=mesh['sp'=8,'tp'=4] {'sp'}, dimensions={0}, use_global_device_ids=true | all-gather | bytes 36864 | tf_op jit(solution)/shard_map/all_gather | solution.py:176
  157.0 3.1 %fusion.12 = f32[1024,512]{1,0:T(8,128)S(1)} fusion(bf16[1024,1024]{1,0:T(8,128)(2,1)} %multiply_convert_fusion, bf16[1,4096,512]{2,1,0:T(8,128)(2,1)} %param.30, s32[]{:T(128)S(6)} %select_n.87), kind=kOutput, calls=%fused_computation.25 | convolution fusion | flops 1073741824 | bytes 5242884 | tf_op jit(solution)/shard_map/dot_general | solution.py:233
  160.2 3.1 %fusion.14 = f32[1024,512]{1,0:T(8,128)S(1)} fusion(bf16[1024,1024]{1,0:T(8,128)(2,1)} %collective-permute-done.12, bf16[2048,512]{1,0:T(8,128)(2,1)} %collective-permute-done.13, s32[]{:T(128)S(6)} %select_n.78), kind=kOutput, calls=%fused_computation.27 | convolution fusion | flops 1073741824 | bytes 5242884 | tf_op jit(solution)/shard_map/dot_general | solution.py:242
  163.3 3.1 %multiply_convert_fusion.1 = bf16[1024,512]{1,0:T(8,128)(2,1)S(1)} fusion(f32[1024,512]{1,0:T(8,128)S(1)} %fusion.14, bf16[1024,1024]{1,0:T(8,128)(2,1)} %multiply_convert_fusion, bf16[2048,512]{1,0:T(8,128)(2,1)} %collective-permute-done.13, s32[]{:T(128)S(6)} %select_n.77, f32[1024]{0:T(1024)S(1)} %bitcast.88), kind=kOutput, calls=%fused_computation.12 | convolution fusion | flops 1075314688 | bytes 6295556 | tf_op jit(solution)/shard_map/dot_general | solution.py:238
  166.4 3.1 %multiply_convert_fusion.2 = bf16[1024,512]{1,0:T(8,128)(2,1)S(1)} fusion(f32[1024,512]{1,0:T(8,128)S(1)} %fusion.12, bf16[1024,1024]{1,0:T(8,128)(2,1)} %collective-permute-done.12, f32[1024]{0:T(1024)S(1)} %bitcast.89, bf16[1,4096,512]{2,1,0:T(8,128)(2,1)} %param.30, s32[]{:T(128)S(6)} %select_n.88), kind=kOutput, calls=%fused_computation.14 | convolution fusion | flops 1075314688 | bytes 6295556 | tf_op jit(solution)/shard_map/dot_general | solution.py:235
  169.5 1.6 pad_maximum_fusion.1
  171.2 0.2 fusion.8
  171.4 0.4 fusion.63
  171.8 0.4 fusion.7
  172.1 5.4 %all_gather.6 = bf16[128,512]{1,0:T(8,128)(2,1)S(1)} all-gather(bf16[128,128]{1,0:T(8,128)(2,1)S(1)} %fusion.7), channel_id=1, replica_groups=mesh['sp'=8,'tp'=4] {'tp'}, dimensions={1}, use_global_device_ids=true | all-gather | bytes 163840 | tf_op jit(solution)/shard_map/all_gather | solution.py:216
  177.6 58.9 %reduce-scatter.2.cloned.1.call-done = bf16[128,1024]{1,0:T(8,128)(2,1)} async-done(((bf16[1024,1024]{1,0:T(8,128)(2,1)}), bf16[128,1024]{1,0:T(8,128)(2,1)}) %reduce-scatter.2.cloned.1.call-update) | async-done | bytes 262160 | tf_op jit(solution)/shard_map/reduce_scatter | solution.py:250
  236.5 0.9 slice.324
  237.4 1.5 collective-permute-start.14
  238.9 0.2 fusion.75
  239.1 3.3 %collective-permute-done.14 = bf16[128,512]{1,0:T(8,128)(2,1)S(1)} collective-permute-done((bf16[128,512]{1,0:T(8,128)(2,1)S(1)}, bf16[128,512]{1,0:T(8,128)(2,1)S(1)}, u32[]{:S(2)}, u32[]{:S(2)}) %collective-permute-start.14) | collective-permute-done | bytes 131104 | tf_op jit(solution)/shard_map/ppermute | solution.py:130
  242.4 1.7 add_convert_fusion.2
  (66 shorter events, 0.7 us)
Async XLA Ops:
  6.5 15.7 %copy-start = (bf16[256,2048]{1,0:T(8,128)(2,1)S(1)}, bf16[256,2048]{1,0:T(8,128)(2,1)}, u32[]{:S(2)}) copy-start(bf16[256,2048]{1,0:T(8,128)(2,1)} %param.24) | copy-start | bytes 3145732
  6.5 15.7 %copy-start.8 = (f32[256]{0:T(256)S(1)}, f32[256]{0:T(256)}, u32[]{:S(2)}) copy-start(f32[256]{0:T(256)} %param.23) | copy-start | bytes 3076
  6.5 15.7 %copy-start.9 = (f32[256]{0:T(256)S(1)}, f32[256]{0:T(256)}, u32[]{:S(2)}) copy-start(f32[256]{0:T(256)} %param.22) | copy-start | bytes 3076
  6.5 229.9 %reduce-scatter.2.cloned.1.call-start = ((), (), s32[]{:S(2)}) async-start(), calls=%async_computation.1 | async-start | bytes 2359296 | tf_op jit(solution)/shard_map/reduce_scatter | solution.py:250
  7.6 6.9 %collective-permute-start = (bf16[30,256]{1,0:T(8,128)(2,1)S(1)}, bf16[30,256]{1,0:T(8,128)(2,1)S(1)}, u32[]{:S(2)}, u32[]{:S(2)}) collective-permute-start(bf16[30,256]{1,0:T(8,128)(2,1)S(1)} %slice.261), channel_id=1, source_target_pairs={{0,4},{4,8},{8,12},{12,16},{16,20},{20,24},{24,28},{1,5},{5,9},{9,... | collective-permute-start | bytes 46088 | tf_op jit(solution)/shard_map/ppermute | solution.py:13
  14.5 18.3 %copy-start.5 = (bf16[128,2048]{1,0:T(8,128)(2,1)S(1)}, bf16[128,2048]{1,0:T(8,128)(2,1)}, u32[]{:S(2)}) copy-start(bf16[128,2048]{1,0:T(8,128)(2,1)} %param.17) | copy-start | bytes 1572868
  22.6 1.6 collective-permute-start.1
  24.3 8.4 %collective-permute-start.2 = (bf16[128,1024]{1,0:T(8,128)(2,1)S(1)}, bf16[128,1024]{1,0:T(8,128)(2,1)S(1)}, u32[]{:S(2)}, u32[]{:S(2)}) collective-permute-start(bf16[128,1024]{1,0:T(8,128)(2,1)S(1)} %add_convert_fusion.1), channel_id=1, source_target_pairs={{0,2},{1,3},{2,0},{3,1},{4,6},{5,7},{6,4},{7,5},{8,10},{9,11},{10,... | collective-permute-start | bytes 786440 | tf_op jit(solution)/shard_map/ppermute | solution.py:130
  32.8 10.2 %collective-permute-start.4 = (bf16[128,1024]{1,0:T(8,128)(2,1)S(1)}, bf16[128,1024]{1,0:T(8,128)(2,1)S(1)}, u32[]{:S(2)}, u32[]{:S(2)}) collective-permute-start(bf16[128,1024]{1,0:T(8,128)(2,1)S(1)} %add_convert_fusion), channel_id=1, source_target_pairs={{0,4},{4,8},{8,12},{12,16},{16,20},{20,24},{24,28},{28,0},{1,5},{5... | collective-permute-start | bytes 786440 | tf_op jit(solution)/shard_map/ppermute | solution.py:200
  43.1 9.3 %collective-permute-start.5 = (bf16[128,1024]{1,0:T(8,128)(2,1)S(1)}, bf16[128,1024]{1,0:T(8,128)(2,1)S(1)}, u32[]{:S(2)}, u32[]{:S(2)}) collective-permute-start(bf16[128,1024]{1,0:T(8,128)(2,1)S(1)} %collective-permute-done.4), channel_id=1, source_target_pairs={{0,4},{4,8},{8,12},{12,16},{16,20},{20,24},{24,28},{28,0},{1,5},{5... | collective-permute-start | bytes 786440 | tf_op jit(solution)/shard_map/ppermute | solution.py:200
  52.4 9.1 %collective-permute-start.6 = (bf16[128,1024]{1,0:T(8,128)(2,1)S(1)}, bf16[128,1024]{1,0:T(8,128)(2,1)S(1)}, u32[]{:S(2)}, u32[]{:S(2)}) collective-permute-start(bf16[128,1024]{1,0:T(8,128)(2,1)S(1)} %collective-permute-done.5), channel_id=1, source_target_pairs={{0,4},{4,8},{8,12},{12,16},{16,20},{20,24},{24,28},{28,0},{1,5},{5... | collective-permute-start | bytes 786440 | tf_op jit(solution)/shard_map/ppermute | solution.py:200
  61.5 9.1 %collective-permute-start.7 = (bf16[128,1024]{1,0:T(8,128)(2,1)S(1)}, bf16[128,1024]{1,0:T(8,128)(2,1)S(1)}, u32[]{:S(2)}, u32[]{:S(2)}) collective-permute-start(bf16[128,1024]{1,0:T(8,128)(2,1)S(1)} %collective-permute-done.6), channel_id=1, source_target_pairs={{0,4},{4,8},{8,12},{12,16},{16,20},{20,24},{24,28},{28,0},{1,5},{5... | collective-permute-start | bytes 786440 | tf_op jit(solution)/shard_map/ppermute | solution.py:200
  70.6 9.7 %collective-permute-start.8 = (bf16[128,1024]{1,0:T(8,128)(2,1)S(1)}, bf16[128,1024]{1,0:T(8,128)(2,1)S(1)}, u32[]{:S(2)}, u32[]{:S(2)}) collective-permute-start(bf16[128,1024]{1,0:T(8,128)(2,1)S(1)} %collective-permute-done.7), channel_id=1, source_target_pairs={{0,4},{4,8},{8,12},{12,16},{16,20},{20,24},{24,28},{28,0},{1,5},{5... | collective-permute-start | bytes 786440 | tf_op jit(solution)/shard_map/ppermute | solution.py:200
  80.2 10.8 %collective-permute-start.9 = (bf16[128,1024]{1,0:T(8,128)(2,1)S(1)}, bf16[128,1024]{1,0:T(8,128)(2,1)S(1)}, u32[]{:S(2)}, u32[]{:S(2)}) collective-permute-start(bf16[128,1024]{1,0:T(8,128)(2,1)S(1)} %collective-permute-done.8), channel_id=1, source_target_pairs={{0,4},{4,8},{8,12},{12,16},{16,20},{20,24},{24,28},{28,0},{1,5},{5... | collective-permute-start | bytes 786440 | tf_op jit(solution)/shard_map/ppermute | solution.py:200
  91.0 9.1 %collective-permute-start.10 = (bf16[128,1024]{1,0:T(8,128)(2,1)S(1)}, bf16[128,1024]{1,0:T(8,128)(2,1)S(1)}, u32[]{:S(2)}, u32[]{:S(2)}) collective-permute-start(bf16[128,1024]{1,0:T(8,128)(2,1)S(1)} %collective-permute-done.9), channel_id=1, source_target_pairs={{0,4},{4,8},{8,12},{12,16},{16,20},{20,24},{24,28},{28,0},{1,5},{5... | collective-permute-start | bytes 786440 | tf_op jit(solution)/shard_map/ppermute | solution.py:200
  91.0 9.8 %collective-permute-start.3 = (bf16[128,1024]{1,0:T(8,128)(2,1)S(1)}, bf16[128,1024]{1,0:T(8,128)(2,1)S(1)}, u32[]{:S(2)}, u32[]{:S(2)}) collective-permute-start(bf16[128,1024]{1,0:T(8,128)(2,1)S(1)} %add_convert_fusion), channel_id=1, source_target_pairs={{0,1},{1,0},{2,3},{3,2},{4,5},{5,4},{6,7},{7,6},{8,9},{9,8},{10,11... | collective-permute-start | bytes 786440 | tf_op jit(solution)/shard_map/ppermute | solution.py:130
  100.1 0.7 copy-start.3
  102.1 2.0 copy-start.1
  105.5 4.5 %collective-permute-start.11 = (bf16[1024,1024]{1,0:T(8,128)(2,1)}, bf16[1024,1024]{1,0:T(8,128)(2,1)}, u32[]{:S(2)}, u32[]{:S(2)}) collective-permute-start(bf16[1024,1024]{1,0:T(8,128)(2,1)} %constant_dynamic-slice_fusion.1), channel_id=1, source_target_pairs={{0,1},{1,0},{2,3},{3,2},{4,5},{5,4},{6,7},{7,6},{8,9},{9,8},{10,11... | collective-permute-start | bytes 6291464 | tf_op jit(solution)/shard_map/ppermute | solution.py:130
  105.5 4.5 %copy-start.2 = (bf16[2048,1024]{1,0:T(8,128)(2,1)S(1)}, bf16[2048,1024]{1,0:T(8,128)(2,1)}, u32[]{:S(2)}) copy-start(bf16[2048,1024]{1,0:T(8,128)(2,1)} %copy-done.1) | copy-start | bytes 12582916
  108.8 51.3 %collective-permute-start.13 = (bf16[2048,512]{1,0:T(8,128)(2,1)}, bf16[2048,512]{1,0:T(8,128)(2,1)}, u32[]{:S(2)}, u32[]{:S(2)}) collective-permute-start(bf16[2048,512]{1,0:T(8,128)(2,1)} %dynamic-slice_bitcast_fusion), channel_id=1, source_target_pairs={{0,2},{1,3},{2,0},{3,1},{4,6},{5,7},{6,4},{7,5},{8,10},{9,11},{10,... | collective-permute-start | bytes 6291464 | tf_op jit(solution)/shard_map/ppermute | solution.py:130
  112.9 2.2 copy-start.10
  112.9 2.2 copy-start.14
  115.1 4.6 %copy-start.11 = (bf16[1,2048,1024]{2,1,0:T(8,128)(2,1)S(1)}, bf16[1,2048,1024]{2,1,0:T(8,128)(2,1)}, u32[]{:S(2)}) copy-start(bf16[1,2048,1024]{2,1,0:T(8,128)(2,1)} %param.29) | copy-start | bytes 12582916
  119.7 6.5 %copy-start.6 = (f32[128,4]{0,1:T(4,128)S(1)}, f32[128,4]{0,1:T(4,128)}, u32[]{:S(2)}) copy-start(f32[128,4]{0,1:T(4,128)} %param.27) | copy-start | bytes 6148
  119.7 6.5 %copy-start.7 = (s32[128,4]{0,1:T(4,128)S(1)}, s32[128,4]{0,1:T(4,128)}, u32[]{:S(2)}) copy-start(s32[128,4]{0,1:T(4,128)} %param.26) | copy-start | bytes 6148
  126.1 34.1 %collective-permute-start.12 = (bf16[1024,1024]{1,0:T(8,128)(2,1)}, bf16[1024,1024]{1,0:T(8,128)(2,1)}, u32[]{:S(2)}, u32[]{:S(2)}) collective-permute-start(bf16[1024,1024]{1,0:T(8,128)(2,1)} %multiply_convert_fusion), channel_id=1, source_target_pairs={{0,1},{1,0},{2,3},{3,2},{4,5},{5,4},{6,7},{7,6},{8,9},{9,8},{10,11... | collective-permute-start | bytes 6291464 | tf_op jit(solution)/shard_map/ppermute | solution.py:130
  169.5 1.9 copy-start.12
  169.5 2.2 copy-start.13
  171.2 67.8 %copy-start.4 = (bf16[512,512]{1,0:T(8,128)(2,1)S(1)}, bf16[512,512]{1,0:T(8,128)(2,1)}, u32[]{:S(2)}) copy-start(bf16[512,512]{1,0:T(8,128)(2,1)} %param.33) | copy-start | bytes 1572868
  237.4 5.0 %collective-permute-start.14 = (bf16[128,512]{1,0:T(8,128)(2,1)S(1)}, bf16[128,512]{1,0:T(8,128)(2,1)S(1)}, u32[]{:S(2)}, u32[]{:S(2)}) collective-permute-start(bf16[128,512]{1,0:T(8,128)(2,1)S(1)} %slice.324), channel_id=1, source_target_pairs={{0,2},{1,3},{2,0},{3,1},{4,6},{5,7},{6,4},{7,5},{8,10},{9,11},{10,... | collective-permute-start | bytes 393224 | tf_op jit(solution)/shard_map/ppermute | solution.py:130
Sparse Core Ops, SparseCore 0:
  171.3 65.1 reduce-scatter.1
